TPU v7x, 32 devices: a whole 2x2x4 slice. The times are simulated.
32 devices in a mesh: ep: 8 (over z, x), tp: 4 (over y, core).
Axes of the slice: x: 2, y: 2, z: 4, core: 2. Of those that a mesh axis runs over, the one named last changes fastest.
Arguments:
- tokens: bfloat16 [1024, 2048], P('ep'), may hold values from -6 to 6
- routes: int32 [1024, 2], P('ep'), may hold values from 0 to 7, all different within a row; in each aligned block of 128 rows (0 to 127, 128 to 255, ...) at most 36 rows name the same one
- route_gates: float32 [1024, 2], P('ep'), may hold values from 0.1 to 2
- cotangent: bfloat16 [1024, 2048], P('ep'), may hold values from -40 to 40
- w_gate: bfloat16 [8, 2048, 1536], P('ep', None, 'tp'), may hold values from -0.125 to 0.125
- w_up: bfloat16 [8, 2048, 1536], P('ep', None, 'tp'), may hold values from -0.125 to 0.125
- w_down: bfloat16 [8, 1536, 2048], P('ep', 'tp'), may hold values from -0.15625 to 0.15625
- s_gate: bfloat16 [2048, 1536], P(None, 'tp'), may hold values from -0.125 to 0.125
- s_up: bfloat16 [2048, 1536], P(None, 'tp'), may hold values from -0.125 to 0.125
- s_down: bfloat16 [1536, 2048], P('tp'), may hold values from -0.15625 to 0.15625
Outputs:
- token_grad: bfloat16 [1024, 2048], P('ep', 'tp')
- gate_grad: float32 [1024, 2], P('ep')
- grad_gate: float32 [8, 2048, 1536], P('ep', None, 'tp')
- grad_up: float32 [8, 2048, 1536], P('ep', None, 'tp')
- grad_down: float32 [8, 1536, 2048], P('ep', 'tp')
- grad_shared: float32 [1536, 2048], P(('tp', 'ep'))
- norm_in: float32 [8, 2, 2048], P('ep')
- norm_down: float32 [8, 1536], P('ep', 'tp')
- norm_shared: float32 [1536], P(('tp', 'ep'))
Inputs may be any that keep to these rules, and one draw needn't show every extreme that they name: `routes`: within the rows of one index of ep no expert is named by more than 36 assignments, a bound that some block reaches.
All inputs are finite; a program needn't handle non-finite values.
Results may differ from a plain program's by a relative error of at most 0.0095.
Values may be sent and summed in bfloat16 or wider, within the bound.
A program may use at most 64 MiB of HBM per device.

v0:
```python
import functools

import jax
import jax.numpy as jnp
from jax import lax
from jax.experimental import pallas as pl
from jax.experimental.pallas import tpu as pltpu
from jax.sharding import PartitionSpec as P

MESH = pl.DeviceIdType.MESH
CORES = 2
BF = jnp.bfloat16
F32 = jnp.float32


def dot(a, b, ca=1, cb=0):
    return lax.dot_general(a, b, (((ca,), (cb,)), ((), ())), preferred_element_type=F32)


def activations(pre_gate, pre_up, hidden_grad):
    sig = jax.nn.sigmoid(pre_gate)
    act = pre_gate * sig
    hidden = (act * pre_up).astype(BF)
    d_gate = (hidden_grad * pre_up * sig * (1.0 + pre_gate * (1.0 - sig))).astype(BF)
    d_up = (hidden_grad * act).astype(BF)
    return hidden, d_gate, d_up


def body(
    ep, tp, cap_pad, live,
    routes, gate_rows, tokens, cot, wg_h, wu_h, wd_h, sg_h, su_h, sd_h,
    token_out, gate_out, shared_out, norm_in_out, norm_down_out, norm_sh_out,
    x_out, c_out, hid_out, dg_out, du_out,
    wg, wu, wd, sg, su, sd, send, rx, acc, prod, term, term_rx, pair, pair_rx,
    part_a, part_own, recv_a, part_b, recv_b, sh_a, sh_own, sh_recv_a, sh_b, sh_recv_b,
    back_tx, back_rx, gpart, grecv, gsend, gback, sq, sq_rx,
    w_sem, out_sem, d1_s, d1_r, d2_s, d2_r, pass_s, rs_s, rs_r, rp_s, rp_r, ra_s, ra_r, rb_s, rb_r,
    bk_s, bk_r, g_s, g_r, gb_s, gb_r, q_s, q_r, sa_s, sa_r, sb_s, sb_r,
):
    me = lax.axis_index("ep")
    j = lax.axis_index("tp")
    core = lax.rem(j, CORES)
    y = lax.div(j, CORES)
    mate = j + 1 - 2 * core
    ny = tp // CORES
    rows = ep * cap_pad
    tok, width = tokens.shape
    share = width // tp
    top = routes.shape[0]
    px = lax.rem(me, 2)
    group = lax.div(me, 2)
    groups = ep // 2
    ff = wg.shape[1]
    sr = shared_out.shape[0]

    loads = [
        pltpu.make_async_copy(src, dst, w_sem.at[n])
        for n, (src, dst) in enumerate(
            [(sg_h, sg), (su_h, su), (sd_h, sd), (wg_h, wg), (wu_h, wu), (wd_h, wd)]
        )
    ]
    for load in loads:
        load.start()

    def ep_peer(step):
        return lax.rem(me + step, ep)

    def remote(src, dst, ssem, rsem, **where):
        copy = pltpu.make_async_remote_copy(
            src_ref=src, dst_ref=dst, send_sem=ssem, recv_sem=rsem,
            device_id=where, device_id_type=MESH,
        )
        copy.start()
        return copy

    barrier = pltpu.get_barrier_semaphore()
    for step in range(1, ep):
        pl.semaphore_signal(barrier, inc=1, device_id={"ep": ep_peer(step)}, device_id_type=MESH)
    for step in range(1, tp):
        pl.semaphore_signal(
            barrier, inc=1, device_id={"tp": lax.rem(j + step, tp)}, device_id_type=MESH
        )

    if live < cap_pad:
        rx[:, :, :, live:, :] = jnp.zeros((tp, 2, ep, cap_pad - live, share), BF)
        back_rx[:, live:, :] = jnp.zeros((ep, cap_pad - live, share), BF)

    sub = lax.broadcasted_iota(jnp.int32, (tok, tok), 0)
    lane = lax.broadcasted_iota(jnp.int32, (tok, tok), 1)

    def to_col(row):
        return jnp.sum(jnp.where(sub == lane, row, 0.0), axis=1, keepdims=True)

    def to_row(col):
        return jnp.sum(jnp.where(sub == lane, col, 0.0), axis=0, keepdims=True)

    expert_row = [routes[k : k + 1, :].astype(F32) for k in range(top)]
    expert_col = [to_col(row) for row in expert_row]
    gate_col = [to_col(gate_rows[k : k + 1, :]) for k in range(top)]
    slot_row = []
    for k in range(top):
        slot = expert_row[k] * cap_pad
        for other in range(top):
            same = (expert_col[other] == expert_row[k]) & (sub < lane)
            slot = slot + jnp.sum(jnp.where(same, 1.0, 0.0), axis=0, keepdims=True)
        slot_row.append(slot)
    slot_col = [to_col(row) for row in slot_row]

    cols = pl.ds(pl.multiple_of(j * share, share), share)
    x_share = tokens[:, cols]
    c_share = cot[:, cols].astype(F32)
    slot_ids = lax.broadcasted_iota(jnp.int32, (rows, tok), 0).astype(F32)
    any_hot = jnp.zeros((rows, tok), F32)
    c_rows = jnp.zeros((rows, share), F32)
    for k in range(top):
        hot = jnp.where(slot_ids == slot_row[k], 1.0, 0.0)
        any_hot = any_hot + hot
        c_rows = c_rows + dot(hot.astype(BF), (gate_col[k] * c_share).astype(BF))
    x_rows = dot(any_hot.astype(BF), x_share)
    send[0] = x_rows.astype(BF).reshape(ep, cap_pad, share)
    send[1] = c_rows.astype(BF).reshape(ep, cap_pad, share)

    pl.semaphore_wait(barrier, ep + tp - 2)

    filled = pl.ds(0, live)
    far_first = sorted(range(1, ep), key=lambda step: -min(step, ep - step))
    waits, d1 = [], {}
    for step in far_first:
        to = ep_peer(step)
        d1[step] = remote(
            send.at[:, to, filled], rx.at[j, :, me, filled], d1_s.at[step], d1_r.at[step], ep=to
        )
        waits.append(d1[step])
    rx[j, :, me] = send[:, me]

    def forward(source):
        block = rx.at[j, :, source, filled]
        remote(block, block, d2_s.at[0], d2_r.at[j], tp=mate)
        for step in range(1, ny):
            to = lax.rem(y + step, ny) * CORES + core
            remote(block, block, d2_s.at[step], d2_r.at[j], tp=to)

    forward(me)

    def part_of(block, d_gate, d_up, gate_w, up_w):
        at = pl.ds(pl.multiple_of(block * share, share), share)
        return dot(d_gate, gate_w[at, :], 1, 1) + dot(d_up, up_w[at, :], 1, 1)

    far_y = [lax.rem(y + step, ny) for step in range(1, ny)] + [y]

    held, sa, rs = {}, [], []

    def shared_gate():
        loads[0].wait()
        held["gate"] = dot(tokens[...], sg[...])

    def shared_up():
        loads[1].wait()
        held["up"] = dot(tokens[...], su[...])

    def shared_act():
        loads[2].wait()
        held["act"] = activations(held["gate"], held["up"], dot(cot[...], sd[...], 1, 1))

    def shared_term(chunks):
        for chunk in chunks:
            at = slice(chunk * share, (chunk + 1) * share)
            value = dot(held["act"][0], cot[:, at], 0, 0)
            for i in range(ep):
                term[i % 2, i // 2, :, at] = value[i * sr : (i + 1) * sr].astype(BF)

    def shared_send():
        for d in range(groups):
            rs.append(
                remote(
                    term.at[1 - px, d], term_rx.at[d], rs_s.at[d], rs_r.at[d],
                    ep=me + 1 - 2 * px,
                )
            )

    def shared_parts():
        for n, yq in enumerate(far_y):
            sh_a[n] = part_of(yq * CORES + 1 - core, *held["act"][1:], sg, su).astype(BF)
            sa.append(remote(sh_a.at[n], sh_recv_a.at[n], sa_s.at[n], sa_r.at[n], tp=mate))

    def shared_own():
        for n, yq in enumerate(far_y):
            sh_own[n] = part_of(yq * CORES + core, *held["act"][1:], sg, su)

    tasks = [
        shared_gate, shared_up, shared_act, lambda: shared_term(range(tp // 2)),
        lambda: (shared_term(range(tp // 2, tp)), shared_send()), shared_parts, shared_own,
    ]
    stride = -(-(ep - 1) // len(tasks))
    for n, task in enumerate(tasks):
        task()
        for step in far_first[n * stride : (n + 1) * stride]:
            d1[step].wait_recv()
            forward(lax.rem(me - step + ep, ep))

    for load in loads[3:]:
        load.wait()
    acc[...] = jnp.zeros_like(acc)

    def add_share(t):
        at = pl.ds(pl.multiple_of(t * share, share), share)
        x_in = rx[t, 0].reshape(rows, share)
        c_in = rx[t, 1].reshape(rows, share)
        acc[0] += dot(x_in, wg[at, :])
        acc[1] += dot(x_in, wu[at, :])
        acc[2] += dot(c_in, wd[:, at], 1, 1)

    def arrived(t):
        pltpu.make_async_remote_copy(
            src_ref=rx.at[t, :, :, filled], dst_ref=rx.at[t, :, :, filled],
            send_sem=d2_s.at[0], recv_sem=d2_r.at[t],
            device_id={"tp": mate}, device_id_type=MESH,
        ).wait_recv()

    add_share(j)
    passed = []
    for step in range(1, ny):
        t = lax.rem(y - step + ny, ny) * CORES + core
        arrived(t)
        whole = rx.at[t, :, :, filled]
        passed.append(remote(whole, whole, pass_s.at[step], d2_r.at[tp + step], tp=mate))
        if step == 1:
            arrived(mate)
            add_share(mate)
        add_share(t)
    for step in range(1, ny):
        t = lax.rem(y - step + ny, ny) * CORES + 1 - core
        passed[step - 1].wait_recv()
        add_share(t)

    rp = []
    for d in range(groups):
        rs[d].wait_recv()
    for step in range(groups):
        d = lax.rem(group + step, groups)
        pair[d] = (term[px, d].astype(F32) + term_rx[d].astype(F32)).astype(BF)
        if step > 0:
            rp.append(
                remote(
                    pair.at[d], pair_rx.at[group], rp_s.at[step], rp_r.at[step], ep=2 * d + px
                )
            )
    pair_rx[group] = pair[group]

    sb = []
    for n, yq in enumerate(far_y[:-1]):
        sa[n].wait_recv()
        sh_b[n] = (sh_own[n] + sh_recv_a[n].astype(F32)).astype(BF)
        sb.append(
            remote(sh_b.at[n], sh_recv_b.at[n], sb_s.at[n], sb_r.at[n], tp=yq * CORES + core)
        )

    outs = []
    for t in range(tp):
        at = pl.ds(t * share, share)
        outs.append(pltpu.make_async_copy(rx.at[t, 0], x_out.at[:, :, at], out_sem.at[2 * t]))
        outs.append(pltpu.make_async_copy(rx.at[t, 1], c_out.at[:, :, at], out_sem.at[2 * t + 1]))
    for out in outs:
        out.start()

    hidden, d_gate, d_up = activations(acc[0], acc[1], acc[2])
    hid_out[...] = hidden
    dg_out[...] = d_gate
    du_out[...] = d_up
    prod[...] = hidden.astype(F32) * acc[2]

    ra = []
    for n, yq in enumerate(far_y):
        value = part_of(yq * CORES + 1 - core, d_gate, d_up, wg, wu).astype(BF)
        part_a[n] = value.reshape(ep, cap_pad, share)
        ra.append(
            remote(part_a.at[n, :, filled], recv_a.at[n, :, filled], ra_s.at[n], ra_r.at[n], tp=mate)
        )
    rb = []
    for n, yq in enumerate(far_y):
        value = part_of(yq * CORES + core, d_gate, d_up, wg, wu)
        part_own[n] = value.reshape(ep, cap_pad, share)
        if n < ny - 1:
            ra[n].wait_recv()
            part_b[n] = (part_own[n] + recv_a[n].astype(F32)).astype(BF)
            rb.append(
                remote(
                    part_b.at[n, :, filled], recv_b.at[n, :, filled], rb_s.at[n], rb_r.at[n],
                    tp=yq * CORES + core,
                )
            )

    gpart[...] = jnp.zeros_like(gpart)
    ones = jnp.ones((8, ff), F32)
    for i in range(ep):
        gpart[i, :, :cap_pad] = lax.dot_general(
            ones, prod[i * cap_pad : (i + 1) * cap_pad, :], (((1,), (1,)), ((), ())),
            preferred_element_type=F32, precision=lax.Precision.HIGHEST,
        )
    gx = []
    for step in range(1, tp):
        gx.append(remote(gpart, grecv.at[step], g_s.at[step], g_r.at[step], tp=lax.rem(j + step, tp)))

    for copy in gx:
        copy.wait_recv()
    total = gpart[...]
    for step in range(1, tp):
        total = total + grecv[step]
    gsend[...] = total.astype(BF).astype(F32)
    gb = []
    for step in range(1, ep):
        to = ep_peer(step)
        gb.append(remote(gsend.at[to], gback.at[me], gb_s.at[step], gb_r.at[step], ep=to))
    gback[me] = gsend[me]

    ra[ny - 1].wait_recv()
    part = part_own[ny - 1] + recv_a[ny - 1].astype(F32)
    for n in range(ny - 1):
        rb[n].wait_recv()
        part = part + recv_b[n].astype(F32)
    back_tx[...] = part.astype(BF)
    bk = []
    for step in range(1, ep):
        to = ep_peer(step)
        bk.append(
            remote(
                back_tx.at[to, filled], back_rx.at[me, filled], bk_s.at[step], bk_r.at[step], ep=to
            )
        )
    back_rx[me, :live] = back_tx[me, :live]

    sa[ny - 1].wait_recv()
    shared_tot = sh_own[ny - 1] + sh_recv_a[ny - 1].astype(F32)
    for n in range(ny - 1):
        sb[n].wait_recv()
        shared_tot = shared_tot + sh_recv_b[n].astype(F32)

    norm_down = jnp.zeros((1, ff), F32)
    for t in range(tp):
        at = slice(t * share, (t + 1) * share)
        x_in = rx[t, 0].reshape(rows, share)
        c_in = rx[t, 1].reshape(rows, share)
        sq[0:1, at] = jnp.sum(jnp.square(dot(dg_out[...], x_in, 0, 0)), axis=0, keepdims=True)
        sq[1:2, at] = jnp.sum(jnp.square(dot(du_out[...], x_in, 0, 0)), axis=0, keepdims=True)
        norm_down += jnp.sum(jnp.square(dot(c_in, hid_out[...], 0, 0)), axis=0, keepdims=True)
    norm_down_out[...] = norm_down / width
    qx = []
    for step in range(1, tp):
        qx.append(remote(sq, sq_rx.at[step], q_s.at[step], q_r.at[step], tp=lax.rem(j + step, tp)))

    for copy in qx:
        copy.wait_recv()
    squares = sq[...]
    for step in range(1, tp):
        squares = squares + sq_rx[step]
    norm_in_out[...] = squares / (tp * ff)

    for copy in rp:
        copy.wait_recv()
    grad = pair_rx[0].astype(F32)
    for i in range(1, groups):
        grad = grad + pair_rx[i].astype(F32)
    shared_out[...] = grad
    norm_sh = jnp.mean(jnp.square(grad), axis=1, keepdims=True)
    here = lax.broadcasted_iota(jnp.int32, (sr, sr), 0) == lax.broadcasted_iota(
        jnp.int32, (sr, sr), 1
    )
    norm_sh_out[...] = jnp.sum(jnp.where(here, norm_sh, 0.0), axis=0, keepdims=True)

    for copy in gb:
        copy.wait_recv()
    spot = lax.broadcasted_iota(jnp.int32, (tok, 128), 1)
    spot_f = spot.astype(F32)
    for k in range(top):
        picked = jnp.zeros((tok, 128), F32)
        for i in range(ep):
            hit = (spot < cap_pad) & (slot_col[k] == spot_f + float(i * cap_pad))
            picked = picked + jnp.where(hit, gback[i, 0:1, :], 0.0)
        dots = to_row(jnp.sum(picked, axis=1, keepdims=True))
        gate_out[k : k + 1, :] = dots / gate_rows[k : k + 1, :]

    place = lax.broadcasted_iota(jnp.int32, (tok, rows), 1).astype(F32)
    pick = jnp.zeros((tok, rows), F32)
    for k in range(top):
        pick = pick + jnp.where(place == slot_col[k], 1.0, 0.0)
    for copy in bk:
        copy.wait_recv()
    token_out[...] = (
        dot(pick.astype(BF), back_rx[...].reshape(rows, share)) + shared_tot
    ).astype(BF)

    sent = rx.at[j, :, :, filled]
    for step in range(ny):
        pltpu.make_async_remote_copy(
            src_ref=sent, dst_ref=sent, send_sem=d2_s.at[step], recv_sem=d2_r.at[j],
            device_id={"tp": mate}, device_id_type=MESH,
        ).wait_send()
    for copy in waits + passed + ra + gx + rb + qx + gb + bk + rs + rp + sa + sb:
        copy.wait_send()
    for out in outs:
        out.wait()


def on_device(
    ep, tp, tokens, routes, route_gates, cotangent, w_gate, w_up, w_down, s_gate, s_up, s_down
):
    tok, width = tokens.shape
    top = routes.shape[1]
    cap = max(2, (9 * tok * top + 8 * ep - 1) // (8 * ep))
    cap_pad = -(-cap // 16) * 16
    rows, share, ff, ny = ep * cap_pad, width // tp, w_gate.shape[2], tp // CORES
    sff = s_gate.shape[1]
    sr = sff // ep

    live = -(-cap // 8) * 8

    vm, hbm = pl.BlockSpec(memory_space=pltpu.VMEM), pl.BlockSpec(memory_space=pl.ANY)
    dma, sds = pltpu.SemaphoreType.DMA, jax.ShapeDtypeStruct
    out_shape = [
        sds((tok, share), BF), sds((top, tok), F32), sds((sr, width), F32), sds((2, width), F32),
        sds((1, ff), F32), sds((1, sr), F32),
        sds((ep, cap_pad, width), BF), sds((ep, cap_pad, width), BF),
        sds((rows, ff), BF), sds((rows, ff), BF), sds((rows, ff), BF),
    ]
    slots = (ny, ep, cap_pad, share)
    scratch = [
        pltpu.VMEM((width, ff), BF), pltpu.VMEM((width, ff), BF), pltpu.VMEM((ff, width), BF),
        pltpu.VMEM((width, sff), BF), pltpu.VMEM((width, sff), BF), pltpu.VMEM((sff, width), BF),
        pltpu.VMEM((2, ep, cap_pad, share), BF),
        pltpu.VMEM((tp, 2, ep, cap_pad, share), BF),
        pltpu.VMEM((3, rows, ff), F32), pltpu.VMEM((rows, ff), F32),
        pltpu.VMEM((2, ep // 2, sr, width), BF), pltpu.VMEM((ep // 2, sr, width), BF),
        pltpu.VMEM((ep // 2, sr, width), BF), pltpu.VMEM((ep // 2, sr, width), BF),
        pltpu.VMEM(slots, BF), pltpu.VMEM(slots, F32), pltpu.VMEM(slots, BF),
        pltpu.VMEM(slots, BF), pltpu.VMEM(slots, BF),
        pltpu.VMEM((ny, tok, share), BF), pltpu.VMEM((ny, tok, share), F32),
        pltpu.VMEM((ny, tok, share), BF), pltpu.VMEM((ny, tok, share), BF),
        pltpu.VMEM((ny, tok, share), BF),
        pltpu.VMEM((ep, cap_pad, share), BF), pltpu.VMEM((ep, cap_pad, share), BF),
        pltpu.VMEM((ep, 8, 128), F32), pltpu.VMEM((tp, ep, 8, 128), F32),
        pltpu.VMEM((ep, 8, 128), F32), pltpu.VMEM((ep, 8, 128), F32),
        pltpu.VMEM((2, width), F32), pltpu.VMEM((tp, 2, width), F32),
        dma((6,)), dma((2 * tp,)), dma((ep,)), dma((ep,)), dma((ny,)), dma((tp + ny,)), dma((ny,)),
        dma((ep,)), dma((ep,)), dma((ep,)), dma((ep,)), dma((ny,)), dma((ny,)), dma((ny,)), dma((ny,)),
        dma((ep,)), dma((ep,)), dma((tp,)), dma((tp,)), dma((ep,)), dma((ep,)), dma((tp,)), dma((tp,)),
        dma((ny,)), dma((ny,)), dma((ny,)), dma((ny,)),
    ]
    out = pl.pallas_call(
        functools.partial(body, ep, tp, cap_pad, live),
        out_shape=out_shape,
        in_specs=[vm] * 4 + [hbm] * 6,
        out_specs=[vm] * 6 + [hbm] * 2 + [vm] * 3,
        scratch_shapes=scratch,
        compiler_params=pltpu.CompilerParams(
            collective_id=0, has_side_effects=True, vmem_limit_bytes=60 * 1024 * 1024
        ),
    )(
        routes.T, route_gates.T, tokens, cotangent,
        w_gate[0], w_up[0], w_down[0], s_gate, s_up, s_down,
    )
    token_grad, gate_grad, grad_shared, norm_in, norm_down, norm_sh, x, c, hid, dg, du = out
    x, c = x.reshape(rows, width), c.reshape(rows, width)
    return (
        token_grad, gate_grad.T, dot(x, dg, 0, 0)[None], dot(x, du, 0, 0)[None],
        dot(hid, c, 0, 0)[None], grad_shared, norm_in[None], norm_down.reshape(1, ff),
        norm_sh.reshape(sr),
    )


def solution(mesh):
    placed = (
        P("ep", None), P("ep", None), P("ep", None), P("ep", None),
        P("ep", None, "tp"), P("ep", None, "tp"), P("ep", "tp", None),
        P(None, "tp"), P(None, "tp"), P("tp", None),
    )
    return jax.shard_map(
        functools.partial(on_device, mesh.shape["ep"], mesh.shape["tp"]),
        mesh=mesh,
        in_specs=placed,
        out_specs=(
            P("ep", "tp"), P("ep", None), P("ep", None, "tp"), P("ep", None, "tp"),
            P("ep", "tp", None), P(("tp", "ep"), None), P("ep", None, None), P("ep", "tp"),
            P(("tp", "ep")),
        ),
        check_vma=False,
    )
```

profile of v0, /device:TPU:0, one launch (start us, length us, event | category | flops | bytes accessed | tf_op | source)
XLA Modules:
  0.0 77.9 jit_solution(9133091976909105431)
XLA Ops:
  0.6 63.6 %shard_map.169 = (bf16[128,512]{1,0:T(8,128)(2,1)}, f32[2,128]{1,0:T(2,128)}, f32[48,2048]{1,0:T(8,128)}, f32[2,2048]{1,0:T(2,128)}, f32[1,384]{1,0:T(1,128)}, /...) custom-call(s32[2,128]{1,0:T(2,128)} %bitcast.29, ...), custom_call_target="tpu_custom_call" | custom-call | tf_op jit(solution)/shard_map/pallas_call | solution.py:448
  64.2 0.0 copy-start
  64.2 0.0 copy-start.4
  64.2 4.4 %convolution_bitcast_fusion.1 = f32[1,2048,384]{2,1,0:T(8,128)} fusion(bf16[384,2048]{1,0:T(8,128)(2,1)} %bitcast.22, bf16[384,384]{1,0:T(8,128)(2,1)} %get-tuple-element.24), kind=kOutput, calls=%fused_computation.1 | convolution fusion | flops 603979776 | bytes 5013504 | tf_op jit(solution)/shard_map/dot_general | solution.py:17
  68.6 0.0 copy-done
  68.6 0.0 copy-done.4
  68.7 0.0 copy-start.1
  68.7 0.0 copy-start.2
  68.7 2.8 %convolution_bitcast_fusion.2 = f32[1,2048,384]{2,1,0:T(8,128)} fusion(bf16[384,2048]{1,0:T(8,128)(2,1)S(1)} %bitcast.23, bf16[384,384]{1,0:T(8,128)(2,1)S(1)} %copy-done.4), kind=kOutput, calls=%fused_computation.2 | convolution fusion | flops 603979776 | bytes 5013504 | tf_op jit(solution)/shard_map/dot_general | solution.py:17
  71.5 0.0 copy-done.1
  71.5 0.0 copy-done.2
  71.5 0.0 copy-start.5
  71.5 0.0 copy-start.8
  71.5 0.0 copy-start.3
  71.5 0.0 copy-start.6
  71.5 0.0 copy-start.7
  71.5 0.0 copy-start.9
  71.6 2.7 %convolution_bitcast_fusion = f32[1,384,2048]{2,1,0:T(8,128)} fusion(bf16[384,384]{1,0:T(8,128)(2,1)S(1)} %copy-done.2, bf16[384,2048]{1,0:T(8,128)(2,1)S(1)} %bitcast.24), kind=kOutput, calls=%fused_computation | convolution fusion | flops 603979776 | bytes 5013504 | tf_op jit(solution)/shard_map/dot_general | solution.py:17
  74.2 0.0 copy-done.5
  74.2 0.7 copy.25
  74.9 0.0 copy-done.8
  74.9 0.6 copy.26
  75.5 0.0 copy-done.3
  75.5 0.7 copy.27
  76.2 0.0 copy-done.6
  76.2 0.6 copy.28
  76.8 0.0 copy-done.7
  76.8 0.6 copy.29
  77.4 0.0 copy-done.9
  77.4 0.5 copy.30
Async XLA Ops:
  64.2 4.4 %copy-start = (bf16[8,48,2048]{2,1,0:T(8,128)(2,1)S(1)}, bf16[8,48,2048]{2,1,0:T(8,128)(2,1)}, u32[]{:S(2)}) copy-start(bf16[8,48,2048]{2,1,0:T(8,128)(2,1)} %get-tuple-element.22) | copy-start | bytes 4718596
  64.2 4.4 %copy-start.4 = (bf16[384,384]{1,0:T(8,128)(2,1)S(1)}, bf16[384,384]{1,0:T(8,128)(2,1)}, u32[]{:S(2)}) copy-start(bf16[384,384]{1,0:T(8,128)(2,1)} %get-tuple-element.23) | copy-start | bytes 884740
  68.7 2.9 %copy-start.1 = (bf16[8,48,2048]{2,1,0:T(8,128)(2,1)S(1)}, bf16[8,48,2048]{2,1,0:T(8,128)(2,1)}, u32[]{:S(2)}) copy-start(bf16[8,48,2048]{2,1,0:T(8,128)(2,1)} %get-tuple-element.26) | copy-start | bytes 4718596
  68.7 2.9 %copy-start.2 = (bf16[384,384]{1,0:T(8,128)(2,1)S(1)}, bf16[384,384]{1,0:T(8,128)(2,1)}, u32[]{:S(2)}) copy-start(bf16[384,384]{1,0:T(8,128)(2,1)} %get-tuple-element.25) | copy-start | bytes 884740
  71.5 2.7 %copy-start.5 = (bf16[128,512]{1,0:T(8,128)(2,1)S(1)}, bf16[128,512]{1,0:T(8,128)(2,1)}, u32[]{:S(2)}) copy-start(bf16[128,512]{1,0:T(8,128)(2,1)} %get-tuple-element.40) | copy-start | bytes 393220
  71.5 3.4 %copy-start.8 = (f32[2,128]{1,0:T(2,128)S(1)}, f32[2,128]{1,0:T(2,128)}, u32[]{:S(2)}) copy-start(f32[2,128]{1,0:T(2,128)} %get-tuple-element.21) | copy-start | bytes 3076
  71.5 3.9 %copy-start.3 = (f32[48,2048]{1,0:T(8,128)S(1)}, f32[48,2048]{1,0:T(8,128)}, u32[]{:S(2)}) copy-start(f32[48,2048]{1,0:T(8,128)} %get-tuple-element.45) | copy-start | bytes 1179652
  71.5 4.7 %copy-start.6 = (f32[2,2048]{1,0:T(2,128)S(1)}, f32[2,2048]{1,0:T(2,128)}, u32[]{:S(2)}) copy-start(f32[2,2048]{1,0:T(2,128)} %get-tuple-element.28) | copy-start | bytes 49156
  71.5 5.3 %copy-start.7 = (f32[1,384]{1,0:T(1,128)S(1)}, f32[1,384]{1,0:T(1,128)}, u32[]{:S(2)}) copy-start(f32[1,384]{1,0:T(1,128)} %get-tuple-element.47) | copy-start | bytes 4612
  71.5 5.8 %copy-start.9 = (f32[1,48]{1,0:T(1,128)S(1)}, f32[1,48]{1,0:T(1,128)}, u32[]{:S(2)}) copy-start(f32[1,48]{1,0:T(1,128)} %get-tuple-element.30) | copy-start | bytes 580
where the time goes:
time: 78.6 us; the launch traced here: 77.9 us
  Pallas kernels  63.6 us (81%)
  matrix products  9.92 us (13%)
  local copies, waits for them, and re-layouts  3.68 us (5%)
    pallas_call x1, Pallas kernels, on_device(): pl.pallas_call(functools.partial(body, ep, tp, cap_pad, live), out_shape=...  63.6 us
    dot_general x3, matrix products, dot(): lax.dot_general(a, b, (((ca,), (cb,)), ((), ())), preferred_element_type=...  9.92 us
    unnamed x26, local copies, waits for them, and re-layouts  3.68 us

commit v1 on v0

v1 whole, which is shorter than its diff:
```python
import functools

import jax
import jax.numpy as jnp
from jax import lax
from jax.experimental import pallas as pl
from jax.experimental.pallas import tpu as pltpu
from jax.sharding import PartitionSpec as P

MESH = pl.DeviceIdType.MESH
CORES = 2
LANES = 128
BF = jnp.bfloat16
F32 = jnp.float32


def dot(a, b, ca=1, cb=0):
    return lax.dot_general(a, b, (((ca,), (cb,)), ((), ())), preferred_element_type=F32)


def activations(pre_gate, pre_up, hidden_grad):
    sig = jax.nn.sigmoid(pre_gate)
    act = pre_gate * sig
    hidden = (act * pre_up).astype(BF)
    d_gate = (hidden_grad * pre_up * sig * (1.0 + pre_gate * (1.0 - sig))).astype(BF)
    d_up = (hidden_grad * act).astype(BF)
    return hidden, d_gate, d_up


def power_of_two(n):
    return n >= 4 and n & (n - 1) == 0


def flip(index, bits):
    place = 1
    while bits >= place:
        if bits & place:
            index = index + place * (1 - 2 * lax.rem(lax.div(index, place), 2))
        place *= 2
    return index


def onward_first(n):
    if n == 1:
        return [0]
    half = onward_first(n // 2)
    return [2 * r + 1 for r in half] + [2 * r for r in half]


def body(
    ep, tp, cap_pad, live,
    routes_h, gate_rows_h, tokens_h, cot_h, wg_h, wu_h, wd_h, sg_h, su_h, sd_h,
    token_out, gate_out, gg_out, gu_out, gd_out, shared_out, norm_in_out, norm_down_out, norm_sh_out,
    routes, gate_rows, tokens, cot, wg, wu, wd, sg, su, sd,
    send, rx, acc, hids, dgs, dus,
    term, half_rx, half_tx, pair, pair_rx,
    part_a, part_own, recv_a, part_b, recv_b, sh_a, sh_own, sh_recv_a, sh_b, sh_recv_b,
    back_tx, back_rx, gsend, gback, gtok, gtok_rx, sq, sq_rx,
    w_sem, d1_s, d1_r, d2_s, d2_r, pass_s, pass_r, ra_s, ra_r, rb_s, rb_r,
    bk_s, bk_r, g_s, g_r, gx_s, gx_r, q_s, q_r, sa_s, sa_r, sb_s, sb_r, h_s, h_r, rp_s, rp_r,
):
    me = lax.axis_index("ep")
    j = lax.axis_index("tp")
    core = lax.rem(j, CORES)
    y = lax.div(j, CORES)
    mate = j + 1 - 2 * core
    ny = tp // CORES
    rows = ep * cap_pad
    tok, width = tokens.shape
    share = width // tp
    top = routes.shape[0]
    ff = wg.shape[1]
    sr = shared_out.shape[0]
    paired = power_of_two(ep)
    batches = 2 if paired else 1
    h = ep // batches
    hrows = h * cap_pad
    filled = pl.ds(0, live)

    def to(m):
        return flip(me, m) if paired else lax.rem(me + m, ep)

    def source(m):
        return flip(me, m) if paired else lax.rem(me - m + ep, ep)

    def block_of(b):
        if batches == 1:
            return pl.ds(0, ep)
        return pl.ds(lax.div(flip(me, b * h), h) * h, h)

    barrier = pltpu.get_barrier_semaphore()
    for m in range(1, ep):
        pl.semaphore_signal(barrier, inc=1, device_id={"ep": to(m)}, device_id_type=MESH)
    for step in range(1, tp):
        pl.semaphore_signal(
            barrier, inc=1, device_id={"tp": lax.rem(j + step, tp)}, device_id_type=MESH
        )

    loads = [
        pltpu.make_async_copy(src, dst, w_sem.at[n])
        for n, (src, dst) in enumerate(
            [
                (routes_h, routes), (gate_rows_h, gate_rows), (tokens_h, tokens), (cot_h, cot),
                (sg_h, sg), (su_h, su), (sd_h, sd), (wg_h, wg), (wu_h, wu), (wd_h, wd),
            ]
        )
    ]
    for load in loads:
        load.start()

    started = []

    def remote(src, dst, ssem, rsem, **where):
        copy = pltpu.make_async_remote_copy(
            src_ref=src, dst_ref=dst, send_sem=ssem, recv_sem=rsem,
            device_id=where, device_id_type=MESH,
        )
        copy.start()
        return copy

    def sent(*args, **where):
        copy = remote(*args, **where)
        started.append(copy)
        return copy

    if live < cap_pad:
        rx[:, :, :, live:, :] = jnp.zeros((tp, 2, ep, cap_pad - live, share), BF)
        back_rx[:, live:, :] = jnp.zeros((ep, cap_pad - live, share), BF)

    sub = lax.broadcasted_iota(jnp.int32, (tok, tok), 0)
    lane = lax.broadcasted_iota(jnp.int32, (tok, tok), 1)

    def to_col(row):
        return jnp.sum(jnp.where(sub == lane, row, 0.0), axis=1, keepdims=True)

    def to_row(col, wide=None):
        n = col.shape[0]
        at = (n, wide or n)
        here = lax.broadcasted_iota(jnp.int32, at, 0) == lax.broadcasted_iota(jnp.int32, at, 1)
        return jnp.sum(jnp.where(here, col, 0.0), axis=0, keepdims=True)

    loads[0].wait()
    loads[1].wait()
    expert_row = [routes[k : k + 1, :].astype(F32) for k in range(top)]
    expert_col = [to_col(row) for row in expert_row]
    gate_col = [to_col(gate_rows[k : k + 1, :]) for k in range(top)]
    slot_row = []
    for k in range(top):
        slot = expert_row[k] * cap_pad
        for other in range(top):
            same = (expert_col[other] == expert_row[k]) & (sub < lane)
            slot = slot + jnp.sum(jnp.where(same, 1.0, 0.0), axis=0, keepdims=True)
        slot_row.append(slot)
    slot_col = [to_col(row) for row in slot_row]

    loads[2].wait()
    loads[3].wait()
    cols = pl.ds(pl.multiple_of(j * share, share), share)
    x_share = tokens[:, cols]
    c_share = cot[:, cols].astype(F32)
    slot_ids = lax.broadcasted_iota(jnp.int32, (rows, tok), 0).astype(F32)
    any_hot = jnp.zeros((rows, tok), F32)
    c_rows = jnp.zeros((rows, share), F32)
    for k in range(top):
        hot = jnp.where(slot_ids == slot_row[k], 1.0, 0.0)
        any_hot = any_hot + hot
        c_rows = c_rows + dot(hot.astype(BF), (gate_col[k] * c_share).astype(BF))
    x_rows = dot(any_hot.astype(BF), x_share)
    send[0] = x_rows.astype(BF).reshape(ep, cap_pad, share)
    send[1] = c_rows.astype(BF).reshape(ep, cap_pad, share)

    pl.semaphore_wait(barrier, ep + tp - 2)

    order = range(1, ep) if paired else sorted(range(1, ep), key=lambda m: -min(m, ep - m))
    d1 = {}
    for m in order:
        dest = to(m)
        d1[m] = sent(
            send.at[:, dest, filled], rx.at[j, :, me, filled], d1_s.at[m], d1_r.at[m], ep=dest
        )
    rx[j, :, me] = send[:, me]

    def forward(origin, b):
        block = rx.at[j, :, origin, filled]
        remote(block, block, d2_s.at[0], d2_r.at[j, b], tp=mate)
        for step in range(1, ny):
            other = lax.rem(y + step, ny) * CORES + core
            remote(block, block, d2_s.at[step], d2_r.at[j, b], tp=other)

    forward(me, 0)

    def pull(ms):
        for m in ms:
            d1[m].wait_recv()
            forward(source(m), m // h)

    def part_of(block, d_gate, d_up, gate_w, up_w):
        at = pl.ds(pl.multiple_of(block * share, share), share)
        return dot(d_gate, gate_w[at, :], 1, 1) + dot(d_up, up_w[at, :], 1, 1)

    far_y = [lax.rem(y + step, ny) for step in range(1, ny)] + [y]

    held, sa, halves, rs, rp = {}, [], {}, [], []

    def shared_act():
        loads[4].wait()
        gate = dot(tokens[...], sg[...])
        loads[5].wait()
        up = dot(tokens[...], su[...])
        loads[6].wait()
        held["act"] = activations(gate, up, dot(cot[...], sd[...], 1, 1))

    def shared_term():
        for chunk in range(tp):
            at = slice(chunk * share, (chunk + 1) * share)
            value = dot(held["act"][0], cot[:, at], 0, 0)
            for i in range(ep):
                term[i, :, at] = value[i * sr : (i + 1) * sr].astype(BF)
        if paired:
            for g in onward_first(ep // 2):
                halves[0, g] = sent(
                    term.at[flip(me, 2 * g + 1)], half_rx.at[g],
                    h_s.at[g], h_r.at[g], ep=flip(me, 1),
                )
        else:
            px = lax.rem(me, 2)
            for d in range(ep // 2):
                rs.append(
                    sent(
                        term.at[2 * d + 1 - px], half_rx.at[d], h_s.at[d], h_r.at[d],
                        ep=me + 1 - 2 * px,
                    )
                )

    def half_slot(stage):
        return ep - (ep >> stage)

    def half_sum(stage, r):
        value = term[flip(me, r << stage)].astype(F32)
        for q in range(stage):
            place = (r << stage) >> (q + 1)
            if (q, place) in halves:
                halves.pop((q, place)).wait_recv()
            value = value + half_rx[half_slot(q) + place].astype(F32)
        return value

    def half_step(stage, r):
        slot = half_slot(stage) + (r >> 1)
        half_tx[slot - ep // 2] = half_sum(stage, r).astype(BF)
        halves[stage, r >> 1] = sent(
            half_tx.at[slot - ep // 2], half_rx.at[slot], h_s.at[slot], h_r.at[slot],
            ep=flip(me, 1 << stage),
        )

    def pair_step():
        px = lax.rem(me, 2)
        group = lax.div(me, 2)
        groups = ep // 2
        for d in range(groups):
            rs[d].wait_recv()
        for step in range(groups):
            d = lax.rem(group + step, groups)
            pair[d] = (term[2 * d + px].astype(F32) + half_rx[d].astype(F32)).astype(BF)
            if step > 0:
                rp.append(
                    sent(
                        pair.at[d], pair_rx.at[group], rp_s.at[step], rp_r.at[step], ep=2 * d + px
                    )
                )
        pair_rx[group] = pair[group]

    def shared_parts():
        for n, yq in enumerate(far_y):
            sh_a[n] = part_of(yq * CORES + 1 - core, *held["act"][1:], sg, su).astype(BF)
            sa.append(sent(sh_a.at[n], sh_recv_a.at[n], sa_s.at[n], sa_r.at[n], tp=mate))

    def shared_own():
        for n, yq in enumerate(far_y):
            sh_own[n] = part_of(yq * CORES + core, *held["act"][1:], sg, su)

    sb = []

    def shared_cross():
        for n, yq in enumerate(far_y[:-1]):
            sa[n].wait_recv()
            sh_b[n] = (sh_own[n] + sh_recv_a[n].astype(F32)).astype(BF)
            sb.append(
                sent(sh_b.at[n], sh_recv_b.at[n], sb_s.at[n], sb_r.at[n], tp=yq * CORES + core)
            )

    def add_share(t, b, first=False):
        at = pl.ds(pl.multiple_of(t * share, share), share)
        blk = block_of(b)
        x_in = rx[t, 0, blk].reshape(hrows, share)
        c_in = rx[t, 1, blk].reshape(hrows, share)
        for n, value in enumerate(
            [dot(x_in, wg[at, :]), dot(x_in, wu[at, :]), dot(c_in, wd[:, at], 1, 1)]
        ):
            value = value.reshape(h, cap_pad, ff)
            acc[n, blk] = value if first else acc[n, blk] + value

    def arrived(t, b):
        block = rx.at[t, :, block_of(b), filled]
        pltpu.make_async_remote_copy(
            src_ref=block, dst_ref=block, send_sem=d2_s.at[0], recv_sem=d2_r.at[t, b],
            device_id={"tp": mate}, device_id_type=MESH,
        ).wait_recv()

    passed = {}

    def gather_near(b):
        add_share(j, b, True)
        arrived(mate, b)
        add_share(mate, b)

    def gather_cross(b):
        for step in range(1, ny):
            t = lax.rem(y - step + ny, ny) * CORES + core
            arrived(t, b)
            block = rx.at[t, :, block_of(b), filled]
            passed[step, b] = sent(block, block, pass_s.at[step, b], pass_r.at[step, b], tp=mate)
            add_share(t, b)

    def gather_last(b):
        for step in range(1, ny):
            passed[step, b].wait_recv()
            add_share(lax.rem(y - step + ny, ny) * CORES + 1 - core, b)

    grads, gs = {}, []

    def activate(b):
        blk = block_of(b)
        parts = [acc[n, blk].reshape(hrows, ff) for n in range(3)]
        hidden, d_gate, d_up = activations(*parts)
        hids[blk] = hidden.reshape(h, cap_pad, ff)
        dgs[blk] = d_gate.reshape(h, cap_pad, ff)
        dus[blk] = d_up.reshape(h, cap_pad, ff)
        grads[b] = d_gate, d_up
        dots = jnp.sum(hidden.astype(F32) * parts[2], axis=1, keepdims=True)
        for s in range(h):
            gsend[blk.start + s] = to_row(dots[s * cap_pad : (s + 1) * cap_pad], LANES)
        for m in range(b * h, (b + 1) * h):
            if m == 0:
                gback[me] = gsend[me]
            else:
                dest = to(m)
                gs.append(sent(gsend.at[dest], gback.at[me], g_s.at[m], g_r.at[m], ep=dest))

    ra, rb = {}, {}

    def parts_mate(b):
        blk = block_of(b)
        for n, yq in enumerate(far_y):
            value = part_of(yq * CORES + 1 - core, *grads[b], wg, wu).astype(BF)
            part_a[n, blk] = value.reshape(h, cap_pad, share)
            ra[n, b] = sent(
                part_a.at[n, blk, filled], recv_a.at[n, blk, filled],
                ra_s.at[n, b], ra_r.at[n, b], tp=mate,
            )

    def parts_own(b):
        blk = block_of(b)
        for n, yq in enumerate(far_y):
            value = part_of(yq * CORES + core, *grads[b], wg, wu)
            part_own[n, blk] = value.reshape(h, cap_pad, share)

    def back_order(b):
        return list(range((b + 1) * h - 1, b * h - 1, -1))

    def cross(b):
        for n in range(ny - 1):
            ra[n, b].wait_recv()
        for m in back_order(b):
            dest = to(m)
            for n in range(ny - 1):
                part_b[n, dest, :live] = (
                    part_own[n, dest, :live] + recv_a[n, dest, :live].astype(F32)
                ).astype(BF)
                rb[n, m] = sent(
                    part_b.at[n, dest, filled], recv_b.at[n, dest, filled],
                    rb_s.at[n, m], rb_r.at[n, m], tp=far_y[n] * CORES + core,
                )

    bk = []

    def back(m):
        b = m // h
        dest = to(m)
        if (ny - 1, b) in ra:
            ra.pop((ny - 1, b)).wait_recv()
        part = part_own[ny - 1, dest, :live] + recv_a[ny - 1, dest, :live].astype(F32)
        for n in range(ny - 1):
            rb[n, m].wait_recv()
            part = part + recv_b[n, dest, :live].astype(F32)
        if m == 0:
            back_rx[me, :live] = part.astype(BF)
        else:
            back_tx[dest, :live] = part.astype(BF)
            bk.append(
                sent(
                    back_tx.at[dest, filled], back_rx.at[me, filled],
                    bk_s.at[m], bk_r.at[m], ep=dest,
                )
            )

    down = []

    def weight_grads(t):
        at = slice(t * share, (t + 1) * share)
        x_in = rx[t, 0].reshape(rows, share)
        c_in = rx[t, 1].reshape(rows, share)
        for n, (out, grad) in enumerate([(gg_out, dgs), (gu_out, dus)]):
            value = dot(x_in, grad[...].reshape(rows, ff), 0, 0)
            out[at, :] = value
            col = jnp.sum(jnp.square(value), axis=1, keepdims=True)
            for i in range(share // LANES):
                lanes = slice(t * share + i * LANES, t * share + (i + 1) * LANES)
                sq[n : n + 1, lanes] = to_row(col[i * LANES : (i + 1) * LANES])
        value = dot(hids[...].reshape(rows, ff), c_in, 0, 0)
        gd_out[:, at] = value
        down.append(jnp.sum(jnp.square(value), axis=1, keepdims=True))

    near, far = list(order)[: h - 1], list(order)[h - 1 :]
    last = batches - 1

    shared_act()
    shared_term()
    pull(near[:1])
    shared_parts()
    pull(near[1:])
    for load in loads[7:]:
        load.wait()
    shared_own()
    if batches > 1:
        gather_near(0)
        pull(far[:1])
        gather_cross(0)
        pull(far[1:2])
        gather_last(0)
        activate(0)
        pull(far[2:3])
        parts_mate(0)
        half_step(1, 3) if ep == 8 else None
        pull(far[3:])
        parts_own(0)
        cross(0)
    gather_near(last)
    gather_cross(last)
    gather_last(last)
    activate(last)
    parts_mate(last)
    parts_own(last)
    cross(last)
    shared_cross()
    if batches > 1:
        for m in back_order(0):
            back(m)
    if paired:
        stage = 1
        while (1 << stage) < ep:
            for r in onward_first(ep >> stage):
                if r % 2 and (stage, r >> 1) not in halves:
                    half_step(stage, r)
            stage += 1
    else:
        pair_step()

    weight_grads(0)
    for m in back_order(last):
        back(m)
    for t in range(1, tp):
        weight_grads(t)
    norm_down_out[...] = to_row(functools.reduce(lambda a, b: a + b, down)) / width
    qx = [
        sent(sq, sq_rx.at[step], q_s.at[step], q_r.at[step], tp=lax.rem(j + step, tp))
        for step in range(1, tp)
    ]

    for copy in gs:
        copy.wait_recv()
    spot = lax.broadcasted_iota(jnp.int32, (tok, LANES), 1)
    spot_f = spot.astype(F32)
    for k in range(top):
        picked = jnp.zeros((tok, LANES), F32)
        for i in range(ep):
            hit = (spot < cap_pad) & (slot_col[k] == spot_f + float(i * cap_pad))
            picked = picked + jnp.where(hit, gback[i], 0.0)
        gtok[k : k + 1, :] = to_row(jnp.sum(picked, axis=1, keepdims=True))
    gx = [
        sent(gtok, gtok_rx.at[step], gx_s.at[step], gx_r.at[step], tp=lax.rem(j + step, tp))
        for step in range(1, tp)
    ]

    if paired:
        stage = 0
        while (1 << stage) < ep:
            stage += 1
        grad = half_sum(stage, 0)
    else:
        for copy in rp:
            copy.wait_recv()
        grad = pair_rx[0].astype(F32)
        for i in range(1, ep // 2):
            grad = grad + pair_rx[i].astype(F32)
    shared_out[...] = grad
    norm_sh_out[...] = to_row(jnp.mean(jnp.square(grad), axis=1, keepdims=True))

    for copy in qx:
        copy.wait_recv()
    squares = sq[...]
    for step in range(1, tp):
        squares = squares + sq_rx[step]
    norm_in_out[...] = squares / (tp * ff)

    for copy in gx:
        copy.wait_recv()
    dots = gtok[...]
    for step in range(1, tp):
        dots = dots + gtok_rx[step]
    gate_out[...] = dots.astype(BF).astype(F32) / gate_rows[...]

    sa[ny - 1].wait_recv()
    shared_tot = sh_own[ny - 1] + sh_recv_a[ny - 1].astype(F32)
    for n in range(ny - 1):
        sb[n].wait_recv()
        shared_tot = shared_tot + sh_recv_b[n].astype(F32)
    place = lax.broadcasted_iota(jnp.int32, (tok, rows), 1).astype(F32)
    pick = jnp.zeros((tok, rows), F32)
    for k in range(top):
        pick = pick + jnp.where(place == slot_col[k], 1.0, 0.0)
    for copy in bk:
        copy.wait_recv()
    token_out[...] = (
        dot(pick.astype(BF), back_rx[...].reshape(rows, share)) + shared_tot
    ).astype(BF)

    forwarded = rx.at[j, :, :, filled]
    for step in range(ny):
        pltpu.make_async_remote_copy(
            src_ref=forwarded, dst_ref=forwarded, send_sem=d2_s.at[step], recv_sem=d2_r.at[j, 0],
            device_id={"tp": mate}, device_id_type=MESH,
        ).wait_send()
    for copy in started:
        copy.wait_send()


def place_out(*refs):
    count = len(refs) // 2
    sem = refs[-1]
    copies = [
        pltpu.make_async_copy(refs[n], refs[count + n], sem.at[n]) for n in range(count)
    ]
    for copy in copies:
        copy.start()
    for copy in copies:
        copy.wait()


def on_device(
    ep, tp, tokens, routes, route_gates, cotangent, w_gate, w_up, w_down, s_gate, s_up, s_down
):
    tok, width = tokens.shape
    top = routes.shape[1]
    cap = max(2, (9 * tok * top + 8 * ep - 1) // (8 * ep))
    cap_pad = -(-cap // 16) * 16
    rows, share, ff, ny = ep * cap_pad, width // tp, w_gate.shape[2], tp // CORES
    sff = s_gate.shape[1]
    sr = sff // ep
    live = -(-cap // 8) * 8
    nb = 2 if power_of_two(ep) else 1
    groups = ep // 2

    vm, hbm = pl.BlockSpec(memory_space=pltpu.VMEM), pl.BlockSpec(memory_space=pl.ANY)
    dma = pltpu.SemaphoreType.DMA
    outs = [
        ((tok, share), BF), ((top, tok), F32), ((width, ff), F32), ((width, ff), F32),
        ((ff, width), F32), ((sr, width), F32), ((2, width), F32), ((1, ff), F32), ((1, sr), F32),
    ]
    slots = (ny, ep, cap_pad, share)
    spare = (1, 16, LANES)
    scratch = [
        pltpu.VMEM((top, tok), jnp.int32), pltpu.VMEM((top, tok), F32),
        pltpu.VMEM((tok, width), BF), pltpu.VMEM((tok, width), BF),
        pltpu.VMEM((width, ff), BF), pltpu.VMEM((width, ff), BF), pltpu.VMEM((ff, width), BF),
        pltpu.VMEM((width, sff), BF), pltpu.VMEM((width, sff), BF), pltpu.VMEM((sff, width), BF),
        pltpu.VMEM((2, ep, cap_pad, share), BF),
        pltpu.VMEM((tp, 2, ep, cap_pad, share), BF),
        pltpu.VMEM((3, ep, cap_pad, ff), F32),
        pltpu.VMEM((ep, cap_pad, ff), BF), pltpu.VMEM((ep, cap_pad, ff), BF),
        pltpu.VMEM((ep, cap_pad, ff), BF),
        pltpu.VMEM((ep, sr, width), BF),
        pltpu.VMEM((ep if nb > 1 else groups, sr, width), BF),
        pltpu.VMEM((groups, sr, width) if nb > 1 else spare, BF),
        pltpu.VMEM(spare if nb > 1 else (groups, sr, width), BF),
        pltpu.VMEM(spare if nb > 1 else (groups, sr, width), BF),
        pltpu.VMEM(slots, BF), pltpu.VMEM(slots, F32), pltpu.VMEM(slots, BF),
        pltpu.VMEM(slots, BF), pltpu.VMEM(slots, BF),
        pltpu.VMEM((ny, tok, share), BF), pltpu.VMEM((ny, tok, share), F32),
        pltpu.VMEM((ny, tok, share), BF), pltpu.VMEM((ny, tok, share), BF),
        pltpu.VMEM((ny, tok, share), BF),
        pltpu.VMEM((ep, cap_pad, share), BF), pltpu.VMEM((ep, cap_pad, share), BF),
        pltpu.VMEM((ep, 1, LANES), F32), pltpu.VMEM((ep, 1, LANES), F32),
        pltpu.VMEM((top, tok), F32), pltpu.VMEM((tp, top, tok), F32),
        pltpu.VMEM((2, width), F32), pltpu.VMEM((tp, 2, width), F32),
        dma((10,)), dma((ep,)), dma((ep,)), dma((ny,)), dma((tp, nb)),
        dma((ny, nb)), dma((ny, nb)), dma((ny, nb)), dma((ny, nb)), dma((ny, ep)), dma((ny, ep)),
        dma((ep,)), dma((ep,)), dma((ep,)), dma((ep,)), dma((tp,)), dma((tp,)), dma((tp,)), dma((tp,)),
        dma((ny,)), dma((ny,)), dma((ny,)), dma((ny,)), dma((ep,)), dma((ep,)), dma((ep,)), dma((ep,)),
    ]
    done = pl.pallas_call(
        functools.partial(body, ep, tp, cap_pad, live),
        out_shape=[pltpu.VMEM(shape, kind) for shape, kind in outs],
        in_specs=[hbm] * 10,
        out_specs=[vm] * 9,
        scratch_shapes=scratch,
        compiler_params=pltpu.CompilerParams(
            collective_id=0, has_side_effects=True, vmem_limit_bytes=48 * 1024 * 1024
        ),
    )(
        routes.T, route_gates.T, tokens, cotangent,
        w_gate[0], w_up[0], w_down[0], s_gate, s_up, s_down,
    )
    out = pl.pallas_call(
        place_out,
        out_shape=[jax.ShapeDtypeStruct(shape, kind) for shape, kind in outs],
        in_specs=[vm] * 9,
        out_specs=[hbm] * 9,
        scratch_shapes=[dma((9,))],
        compiler_params=pltpu.CompilerParams(vmem_limit_bytes=8 * 1024 * 1024),
    )(*[pltpu.with_memory_space_constraint(value, pltpu.VMEM) for value in done])
    token_grad, gate_grad, gg, gu, gd, grad_shared, norm_in, norm_down, norm_sh = out
    return (
        token_grad, gate_grad.T, gg[None], gu[None], gd[None], grad_shared, norm_in[None],
        norm_down.reshape(1, ff), norm_sh.reshape(sr),
    )


def solution(mesh):
    placed = (
        P("ep", None), P("ep", None), P("ep", None), P("ep", None),
        P("ep", None, "tp"), P("ep", None, "tp"), P("ep", "tp", None),
        P(None, "tp"), P(None, "tp"), P("tp", None),
    )
    return jax.shard_map(
        functools.partial(on_device, mesh.shape["ep"], mesh.shape["tp"]),
        mesh=mesh,
        in_specs=placed,
        out_specs=(
            P("ep", "tp"), P("ep", None), P("ep", None, "tp"), P("ep", None, "tp"),
            P("ep", "tp", None), P(("tp", "ep"), None), P("ep", None, None), P("ep", "tp"),
            P(("tp", "ep")),
        ),
        check_vma=False,
    )
```

time: 78.6 us -> 53.6 us (0.68)
  Pallas kernels: 63.6 us -> 52.6 us
  matrix products: 9.92 us -> 0 us
  local copies, waits for them, and re-layouts: 3.68 us -> 0 us
    pallas_call x1, Pallas kernels: 63.6 us -> 48.7 us  [on_device(): pl.pallas_call(functools.partial(body, ep, tp, cap_pad, live), out_shape=...]
    dot_general x3 -> x0, matrix products: 9.92 us -> none  [dot(): lax.dot_general(a, b, (((ca,), (cb,)), ((), ())), preferred_element_type=...]
    pallas_call x0 -> x1, Pallas kernels: none -> 3.9 us  [on_device(): pl.pallas_call(place_out, out_shape=[jax.ShapeDtypeStruct(shape, kind) fo...]
    unnamed x26 -> x0, local copies, waits for them, and re-layouts: 3.68 us -> none
where the time goes in v1:
time: 53.6 us; the launch traced here: 53.3 us
  Pallas kernels  52.6 us (98%)
  between operations  0.65 us (1%)
    pallas_call x1, Pallas kernels, on_device(): pl.pallas_call(functools.partial(body, ep, tp, cap_pad, live), out_shape=...  48.7 us
    pallas_call x1, Pallas kernels, on_device(): pl.pallas_call(place_out, out_shape=[jax.ShapeDtypeStruct(shape, kind) fo...  3.9 us

profile of v1, /device:TPU:0, one launch (start us, length us, event | category | flops | bytes accessed | tf_op | source)
XLA Modules:
  0.0 53.3 jit_solution(13323560855574378710)
XLA Ops:
  0.6 48.7 %shard_map.169 = (bf16[128,512]{1,0:T(8,128)(2,1)S(1)}, f32[2,128]{1,0:T(2,128)S(1)}, f32[2048,384]{1,0:T(8,128)S(1)}, f32[2048,384]{1,0:T(8,128)S(1)}, f32[384,...) custom-call(s32[2,128]{1,0:T(2,128)} %bitcast.14, ...), custom_call_target="tpu_custom_call" | custom-call | tf_op jit(solution)/shard_map/pallas_call | solution.py:610
  49.4 3.9 %shard_map.170 = (bf16[128,512]{1,0:T(8,128)(2,1)}, f32[2,128]{1,0:T(2,128)}, f32[2048,384]{1,0:T(8,128)}, f32[2048,384]{1,0:T(8,128)}, f32[384,2048]{1,0:T(8,12...) custom-call(bf16[128,512]{1,0:T(8,128)(2,1)S(1)} %get-tuple-element.27.refs_0_, ...), custom_call_target="tpu_custom_call" | custom-call | tf_op jit(solution)/shard_map/pallas_call | solution.py:623
